TPU v7x, 32 devices: a whole 2x2x4 slice. The times are simulated.
32 devices in a mesh: kv: 8 (over z, y), tp: 4 (over x, core).
Axes of the slice: x: 2, y: 2, z: 4, core: 2. Of those that a mesh axis runs over, the one named last changes fastest.
Arguments:
- residual_in: bfloat16 [64, 2048], P(None, ('kv', 'tp')), may hold values from -14 to 14
- delta_state: float32 [64, 32, 128, 128], P('kv', 'tp'), may hold values from -1 to 1
- norm_gain_first: float32 [2048], P('kv'), may hold values from 0.1 to 1.9
- gate_first: bfloat16 [2048, 5632], P('kv', 'tp'), may hold values from -0.125 to 0.125
- up_first: bfloat16 [2048, 5632], P('kv', 'tp'), may hold values from -0.125 to 0.125
- down_first: bfloat16 [5632, 2048], P('tp', 'kv'), may hold values from -0.15625 to 0.15625
- norm_gain_mixer: float32 [2048], P('kv'), may hold values from 0.1 to 1.9
- query_weight: bfloat16 [2048, 2048], P('kv', 'tp'), may hold values from -0.125 to 0.125
- key_weight: bfloat16 [2048, 2048], P('kv', 'tp'), may hold values from -0.125 to 0.125
- value_weight: bfloat16 [2048, 4096], P('kv', 'tp'), may hold values from -0.125 to 0.125
- output_gate_weight: bfloat16 [2048, 4096], P('kv', 'tp'), may hold values from -0.125 to 0.125
- beta_weight: bfloat16 [2048, 32], P('kv'), may hold values from -0.125 to 0.125
- decay_weight: bfloat16 [2048, 32], P('kv'), may hold values from -0.125 to 0.125
- decay_rate: float32 [32], P('tp'), may hold values from -2.3 to 1.1
- decay_bias: float32 [32], P('tp'), may hold values from -1 to 1
- head_gain: float32 [128], replicated, may hold values from 0.1 to 1.9
- out_weight: bfloat16 [4096, 2048], P('tp', 'kv'), may hold values from -0.125 to 0.125
- norm_gain_second: float32 [2048], P('kv'), may hold values from 0.1 to 1.9
- gate_second: bfloat16 [2048, 5632], P('kv', 'tp'), may hold values from -0.125 to 0.125
- up_second: bfloat16 [2048, 5632], P('kv', 'tp'), may hold values from -0.125 to 0.125
- down_second: bfloat16 [5632, 2048], P('tp', 'kv'), may hold values from -0.15625 to 0.15625
Outputs:
- residual_out: bfloat16 [64, 2048], P(None, ('kv', 'tp'))
- delta_state_out: float32 [64, 32, 128, 128], P('kv', 'tp')
All inputs are finite; a program needn't handle non-finite values.
Results may differ from a plain program's by a relative error of at most 0.03.
Values may be sent and summed in bfloat16 or wider, within the bound.
A program may use at most 64 MiB of HBM per device.

v0:
```python
import functools

import jax
import jax.numpy as jnp
from jax import lax
from jax.experimental import pallas as pl
from jax.experimental.pallas import tpu as pltpu
from jax.sharding import PartitionSpec as P

EPS = 1e-06
LANES = 128
BF16 = jnp.bfloat16
F32 = jnp.float32


def pad_lanes(size):
    return -(-size // LANES) * LANES


def silu(v):
    return v / (1.0 + jnp.exp(-v))


def dot(a, b):
    return jnp.dot(a, b, preferred_element_type=F32)


def dot_first(a, b):
    return lax.dot_general(a, b, (((0,), (0,)), ((), ())), preferred_element_type=F32)


def place(rows, cols, shift):
    row = lax.broadcasted_iota(jnp.int32, (rows, cols), 0)
    col = lax.broadcasted_iota(jnp.int32, (rows, cols), 1)
    return jnp.where(col == row + shift, 1.0, 0.0).astype(F32).astype(BF16)


def kernel(
    n_kv,
    n_tp,
    res_ref,
    gain_first_ref,
    gain_mixer_ref,
    gain_second_ref,
    beta_ref,
    decay_ref,
    rate_ref,
    bias_ref,
    head_gain_ref,
    state_hbm,
    gate1_hbm,
    up1_hbm,
    down1_hbm,
    wq_hbm,
    wk_hbm,
    wv_hbm,
    wo_hbm,
    out_hbm,
    gate2_hbm,
    up2_hbm,
    down2_hbm,
    res_out_ref,
    state_out_hbm,
    gate1,
    up1,
    down1,
    wq,
    wk,
    wv,
    wo,
    wout,
    gate2,
    up2,
    down2,
    state,
    res_all,
    s1a,
    r1a,
    s1b,
    r1b,
    hid1,
    par1,
    sma,
    rma,
    smb,
    rmb,
    smc,
    rmc,
    nrm,
    parm,
    s2a,
    r2a,
    s2b,
    r2b,
    hid2,
    fin_send,
    fin_recv,
    qk_rows,
    val_rows,
    beta_rows,
    dec_rows,
    read_rows,
    w_sem,
    in_sem,
    out_sem,
    send_sem,
    recv_sem,
):
    kv = lax.axis_index("kv")
    tp = lax.axis_index("tp")
    batch, piece = res_ref.shape
    depth = gate1.shape[0]
    width = depth * n_kv
    own_rows = batch // n_kv
    heads = state.shape[1]
    size = state.shape[2]
    key_cols = wq.shape[1]
    key_heads = key_cols // size
    repeat = heads // key_heads
    val_cols = wv.shape[1]

    weight_pairs = (
        (gate1_hbm, gate1),
        (up1_hbm, up1),
        (down1_hbm, down1),
        (wq_hbm, wq),
        (wk_hbm, wk),
        (wv_hbm, wv),
        (wo_hbm, wo),
        (out_hbm, wout),
        (gate2_hbm, gate2),
        (up2_hbm, up2),
        (down2_hbm, down2),
    )
    loads = [
        pltpu.make_async_copy(src, dst, w_sem.at[i]) for i, (src, dst) in enumerate(weight_pairs)
    ]
    for load in loads[:7]:
        load.start()

    barrier = pltpu.get_barrier_semaphore()
    for off in range(1, n_tp):
        pl.semaphore_signal(
            barrier,
            inc=1,
            device_id={"tp": lax.rem(tp + off, n_tp)},
            device_id_type=pl.DeviceIdType.MESH,
        )
    for off in range(1, n_kv):
        pl.semaphore_signal(
            barrier,
            inc=1,
            device_id={"kv": lax.rem(kv + off, n_kv)},
            device_id_type=pl.DeviceIdType.MESH,
        )
    pl.semaphore_wait(barrier, n_tp - 1 + n_kv - 1)

    pending = []

    def send(event, off, src, dst, axis, peer):
        copy = pltpu.make_async_remote_copy(
            src_ref=src,
            dst_ref=dst,
            send_sem=send_sem.at[event, off],
            recv_sem=recv_sem.at[event, off],
            device_id={axis: peer},
            device_id_type=pl.DeviceIdType.MESH,
        )
        copy.start()
        pending.append(copy)
        return copy

    def gather(event, axis, me, count, own, slots):
        return [
            send(event, off, own, slots.at[me], axis, lax.rem(me + off, count))
            for off in range(1, count)
        ]

    def scatter(event, sends, receives):
        copies = []
        for off in range(1, n_kv):
            peer = lax.rem(kv + off, n_kv)
            copies.append(send(event, off, sends.at[peer], receives.at[kv], "kv", peer))
        return copies

    def collect(copies, sends, receives):
        total = sends[kv].astype(F32)
        for off in range(1, n_kv):
            copies[off - 1].wait_recv()
            source = lax.rem(kv + n_kv - off, n_kv)
            total = total + receives[source].astype(F32)
        return total

    def put(ref, offset, value):
        cols = value.shape[1]
        ref[:, :, offset : offset + cols] = value.reshape(n_kv, own_rows, cols).astype(BF16)

    def square_lanes(residual):
        squares = jnp.sum(residual * residual, axis=1, keepdims=True)
        high = squares.astype(BF16).astype(F32)
        lane = lax.broadcasted_iota(jnp.int32, (batch, LANES), 1)
        return jnp.where(lane == 64, high, jnp.where(lane == 65, squares - high, 0.0))

    def row_scale(extra):
        squares = extra[:, 64:65] + extra[:, 65:66]
        return lax.rsqrt(squares / width + EPS)

    def flat(slots):
        both = slots[...].astype(F32)
        return both.reshape(batch, both.shape[2]).astype(BF16)

    def exchange(event, value, slots):
        slots[tp] = value.astype(BF16)
        copies = gather(event, "tp", tp, n_tp, slots.at[tp], slots)
        for copy in copies:
            copy.wait_recv()
        total = slots[0].astype(F32)
        for other in range(1, n_tp):
            total = total + slots[other].astype(F32)
        return total

    def half_ffn(event, residual, gain_ref, first, w_gate, w_up, w_down, bufs, hid):
        send_a, recv_a, send_b, recv_b = bufs
        hidden_cols = w_gate.shape[1]
        up_end = pad_lanes(hidden_cols)
        scaled = (residual * gain_ref[...]).astype(BF16)
        loads[first].wait()
        put(send_a, 0, dot(scaled, w_gate[...]))
        copies_a = scatter(event, send_a, recv_a)
        loads[first + 1].wait()
        put(send_b, 0, dot(scaled, w_up[...]))
        put(send_b, up_end, square_lanes(residual))
        copies_b = scatter(event + 1, send_b, recv_b)
        gate_sum = collect(copies_a, send_a, recv_a)[:, :hidden_cols]
        rest = collect(copies_b, send_b, recv_b)
        scale = row_scale(rest[:, up_end:])
        hidden = (silu(gate_sum * scale) * (rest[:, :hidden_cols] * scale)).astype(BF16)
        hid[kv] = hidden
        copies = gather(event + 2, "kv", kv, n_kv, hid.at[kv], hid)
        loads[first + 2].wait()
        for copy in copies:
            copy.wait_recv()
        return dot(flat(hid), w_down[...])

    copies = gather(0, "tp", tp, n_tp, res_ref, res_all)
    for load in loads[7:]:
        load.start()
    for row in range(own_rows):
        pltpu.make_async_copy(state_hbm.at[row], state.at[row], in_sem.at[row]).start()
    decay_exp = jnp.exp(rate_ref[...])
    extra_weight = (
        dot_first(beta_ref[...], place_heads(beta_ref.shape[0], tp * heads, 0, heads))
        + dot_first(decay_ref[...], place_heads(beta_ref.shape[0], tp * heads, heads, heads))
    ).astype(BF16)
    residual = dot(res_ref[...], place(piece, depth, tp * piece))
    for off in range(1, n_tp):
        copies[off - 1].wait_recv()
        source = lax.rem(tp + n_tp - off, n_tp)
        residual = residual + dot(res_all[source], place(piece, depth, source * piece))

    product = half_ffn(
        1, residual, gain_first_ref, 0, gate1, up1, down1, (s1a, r1a, s1b, r1b), hid1
    )
    branch = exchange(4, product, par1)
    after_first = (residual + 0.5 * branch).astype(BF16).astype(F32)

    scaled = (after_first * gain_mixer_ref[...]).astype(BF16)
    loads[3].wait()
    put(sma, 0, dot(scaled, wq[...]))
    loads[4].wait()
    put(sma, key_cols, dot(scaled, wk[...]))
    put(sma, 2 * key_cols, dot(scaled, extra_weight) + square_lanes(after_first))
    copies_a = scatter(5, sma, rma)
    loads[5].wait()
    put(smb, 0, dot(scaled, wv[...]))
    copies_b = scatter(6, smb, rmb)
    loads[6].wait()
    put(smc, 0, dot(scaled, wo[...]))
    copies_c = scatter(7, smc, rmc)

    keys_sum = collect(copies_a, sma, rma)
    extra = keys_sum[:, 2 * key_cols :]
    scale = row_scale(extra)
    for head in range(key_heads):
        for slot, start, factor in (
            (head, head * size, size ** (-0.5)),
            (key_heads + head, key_cols + head * size, 1.0),
        ):
            act = silu(keys_sum[:, start : start + size] * scale)
            unit = act * lax.rsqrt(jnp.sum(act * act, axis=1, keepdims=True) + EPS)
            qk_rows[:, slot, :] = unit * factor
    gates = extra * scale
    beta_pre = gates[:, :heads]
    decay_pre = gates[:, heads : 2 * heads] + bias_ref[...]
    beta_gate = 1.0 / (1.0 + jnp.exp(-beta_pre))
    softplus = jnp.maximum(decay_pre, 0.0) + jnp.log1p(jnp.exp(-jnp.abs(decay_pre)))
    decay_gate = jnp.exp(-decay_exp * softplus)
    for head in range(heads):
        beta_rows[:, head, :] = jnp.broadcast_to(beta_gate[:, head : head + 1], (own_rows, size))
        dec_rows[:, head, :] = jnp.broadcast_to(decay_gate[:, head : head + 1], (own_rows, size))
    values = silu(collect(copies_b, smb, rmb) * scale)
    for head in range(heads):
        val_rows[:, head, :] = values[:, head * size : (head + 1) * size]

    def step(row, carry):
        pltpu.make_async_copy(state_hbm.at[row], state.at[row], in_sem.at[row]).wait()
        columns = qk_rows[row].T
        row_vals, row_beta, row_dec = val_rows[row], beta_rows[row], dec_rows[row]
        for head in range(heads):
            kh = head // repeat
            key_col = columns[:, key_heads + kh : key_heads + kh + 1]
            query_col = columns[:, kh : kh + 1]
            faded = state[row, head] * row_dec[head : head + 1, :]
            predicted = jnp.sum(faded * key_col, axis=0, keepdims=True)
            correction = row_beta[head : head + 1, :] * (row_vals[head : head + 1, :] - predicted)
            updated = faded + key_col * correction
            state[row, head] = updated
            read_rows[row, head : head + 1, :] = jnp.sum(updated * query_col, axis=0, keepdims=True)
        pltpu.make_async_copy(state.at[row], state_out_hbm.at[row], out_sem.at[row]).start()
        return carry

    lax.fori_loop(0, own_rows, step, 0)

    out_gate = silu(collect(copies_c, smc, rmc) * scale)
    for head in range(heads):
        reading = read_rows[:, head, :]
        mean = jnp.mean(reading * reading, axis=1, keepdims=True)
        normed = reading * lax.rsqrt(mean + EPS) * head_gain_ref[...]
        cols = slice(head * size, (head + 1) * size)
        nrm[kv, :, cols] = (normed * out_gate[:, cols]).astype(BF16)
    copies = gather(8, "kv", kv, n_kv, nrm.at[kv], nrm)
    loads[7].wait()
    for copy in copies:
        copy.wait_recv()
    branch = exchange(9, dot(flat(nrm), wout[...]), parm)
    after_mixer = (after_first + branch).astype(BF16).astype(F32)

    product = half_ffn(
        10, after_mixer, gain_second_ref, 8, gate2, up2, down2, (s2a, r2a, s2b, r2b), hid2
    ).astype(BF16)
    copies = []
    for off in range(1, n_tp):
        peer = lax.rem(tp + off, n_tp)
        fin_send[off] = dot(product, place_back(depth, piece, peer)).astype(BF16)
        copies.append(send(13, off, fin_send.at[off], fin_recv.at[off], "tp", peer))
    mine = place_back(depth, piece, tp)
    own_cols = dot(after_mixer.astype(BF16), mine)
    branch = dot(product, mine)
    for off in range(1, n_tp):
        copies[off - 1].wait_recv()
        branch = branch + fin_recv[off].astype(F32)
    res_out_ref[...] = (own_cols + 0.5 * branch).astype(BF16)

    for copy in pending:
        copy.wait_send()

    def drain(row, carry):
        pltpu.make_async_copy(state.at[row], state_out_hbm.at[row], out_sem.at[row]).wait()
        return carry

    lax.fori_loop(0, own_rows, drain, 0)


def place_back(rows, cols, peer):
    row = lax.broadcasted_iota(jnp.int32, (rows, cols), 0)
    col = lax.broadcasted_iota(jnp.int32, (rows, cols), 1)
    return jnp.where(row == col + peer * cols, 1.0, 0.0).astype(F32).astype(BF16)


def place_heads(rows, first, lane_start, count):
    row = lax.broadcasted_iota(jnp.int32, (rows, LANES), 0)
    col = lax.broadcasted_iota(jnp.int32, (rows, LANES), 1)
    inside = (col >= lane_start) & (col < lane_start + count)
    hit = inside & (row == col - lane_start + first)
    return jnp.where(hit, 1.0, 0.0).astype(F32).astype(BF16)


def body(
    n_kv,
    n_tp,
    residual_in,
    delta_state,
    norm_gain_first,
    gate_first,
    up_first,
    down_first,
    norm_gain_mixer,
    query_weight,
    key_weight,
    value_weight,
    output_gate_weight,
    beta_weight,
    decay_weight,
    decay_rate,
    decay_bias,
    head_gain,
    out_weight,
    norm_gain_second,
    gate_second,
    up_second,
    down_second,
):
    batch, piece = residual_in.shape
    depth, hidden = gate_first.shape
    own_rows, heads, size, _ = delta_state.shape
    key_cols = query_weight.shape[1]
    val_cols = value_weight.shape[1]
    key_heads = key_cols // size
    hp = pad_lanes(hidden)

    def like(x):
        return pltpu.VMEM(x.shape, x.dtype)

    def slots(cols):
        return pltpu.VMEM((n_kv, own_rows, cols), BF16)

    def row_buf(count):
        return pltpu.VMEM((own_rows, count, size), F32)

    tp_slots = pltpu.VMEM((n_tp, batch, depth), BF16)
    ffn_bufs = [slots(hp)] * 2 + [slots(hp + LANES)] * 2 + [slots(hidden), tp_slots]
    mixer_bufs = (
        [slots(2 * key_cols + LANES)] * 2
        + [slots(val_cols)] * 4
        + [slots(heads * size), tp_slots]
    )
    big = (
        gate_first,
        up_first,
        down_first,
        query_weight,
        key_weight,
        value_weight,
        output_gate_weight,
        out_weight,
        gate_second,
        up_second,
        down_second,
    )
    small = (
        residual_in,
        norm_gain_first[None, :],
        norm_gain_mixer[None, :],
        norm_gain_second[None, :],
        beta_weight.T,
        decay_weight.T,
        decay_rate[None, :],
        decay_bias[None, :],
        head_gain[None, :],
    )
    vmem = pl.BlockSpec(memory_space=pltpu.VMEM)
    hbm = pl.BlockSpec(memory_space=pl.ANY)
    most = max(n_kv, n_tp)
    return pl.pallas_call(
        functools.partial(kernel, n_kv, n_tp),
        out_shape=(
            jax.ShapeDtypeStruct(residual_in.shape, BF16),
            jax.ShapeDtypeStruct(delta_state.shape, F32),
        ),
        in_specs=[vmem] * len(small) + [hbm] * (1 + len(big)),
        out_specs=(vmem, hbm),
        scratch_shapes=[like(x) for x in big]
        + [like(delta_state), pltpu.VMEM((n_tp, batch, piece), BF16)]
        + ffn_bufs
        + mixer_bufs
        + ffn_bufs[:-1]
        + [pltpu.VMEM((n_tp, batch, piece), BF16)] * 2
        + [row_buf(2 * key_heads), row_buf(heads), row_buf(heads), row_buf(heads), row_buf(heads)]
        + [
            pltpu.SemaphoreType.DMA((len(big),)),
            pltpu.SemaphoreType.DMA((own_rows,)),
            pltpu.SemaphoreType.DMA((own_rows,)),
            pltpu.SemaphoreType.DMA((14, most)),
            pltpu.SemaphoreType.DMA((14, most)),
        ],
        compiler_params=pltpu.CompilerParams(
            collective_id=0, has_side_effects=True, vmem_limit_bytes=60 * 1024 * 1024
        ),
        name="layer",
    )(*small, delta_state, *big)


def solution(mesh):
    placed = (
        P(None, ("kv", "tp")),
        P("kv", "tp", None, None),
        P("kv"),
        P("kv", "tp"),
        P("kv", "tp"),
        P("tp", "kv"),
        P("kv"),
        P("kv", "tp"),
        P("kv", "tp"),
        P("kv", "tp"),
        P("kv", "tp"),
        P("kv", None),
        P("kv", None),
        P("tp"),
        P("tp"),
        P(),
        P("tp", "kv"),
        P("kv"),
        P("kv", "tp"),
        P("kv", "tp"),
        P("tp", "kv"),
    )
    return jax.shard_map(
        functools.partial(body, mesh.shape["kv"], mesh.shape["tp"]),
        mesh=mesh,
        in_specs=placed,
        out_specs=(P(None, ("kv", "tp")), P("kv", "tp", None, None)),
        check_vma=False,
    )
```

profile of v0, /device:TPU:0, one launch (start us, length us, event | category | flops | bytes accessed | tf_op | source)
XLA Modules:
  0.0 78.9 jit_solution(5585662020206882538)
XLA Ops:
  0.6 72.2 %layer.1 = (bf16[64,64]{1,0:T(8,128)(2,1)}, f32[8,8,128,128]{3,2,1,0:T(8,128)}) custom-call(bf16[64,64]{1,0:T(8,128)(2,1)} %res_ref.1, f32[1,256]{1,0:T(1,128)} %bitcast.10, f32[1,256]{1,0:T(1,128)} %bitcast.11, f32[1,256]{1,0:T(1,128)} %bitcast.12, bf16[32,256]{1,0:T(8,128)(2,1)} %bitcast.8, bf16[32,256]{1,0:T(8,128)(2,1)} %bitcast.9, f32[1,8]{1,0:T(1,128)} %bitcast.13, ...), custom_call_target="tpu_custom_call" | custom-call | tf_op jit(solution)/shard_map/layer/pallas_call | solution.py:454
  72.8 1.3 %copy.25 = bf16[64,64]{1,0:T(8,128)(2,1)} copy(bf16[64,64]{1,0:T(8,128)(2,1)} %get-tuple-element.4) | data formatting | bytes 16384
  74.2 4.7 %copy.26 = f32[8,8,128,128]{3,2,1,0:T(8,128)} copy(f32[8,8,128,128]{3,2,1,0:T(8,128)} %get-tuple-element.5) | data formatting | bytes 8388608
where the time goes:
time: 79.1 us; the launch traced here: 78.9 us
  Pallas kernels  72.2 us (91%)
  local copies, waits for them, and re-layouts  6.02 us (8%)
    pallas_call x1, Pallas kernels, body(): pl.pallas_call(functools.partial(kernel, n_kv, n_tp), out_shape=(jax.Shap...  72.2 us
    unnamed x2, local copies, waits for them, and re-layouts  6.02 us

commit v1 on v0

v1 whole, which is shorter than its diff:
```python
import functools

import jax
import jax.numpy as jnp
from jax import lax
from jax.experimental import pallas as pl
from jax.experimental.pallas import tpu as pltpu
from jax.sharding import PartitionSpec as P

EPS = 1e-06
GROUP = 8
LANES = 128
BF16 = jnp.bfloat16
F32 = jnp.float32
ns = jax.named_scope


def pad_lanes(size):
    return -(-size // LANES) * LANES


def silu(v):
    return v / (1.0 + jnp.exp(-v))


def dot(a, b):
    return jnp.dot(a, b, preferred_element_type=F32)


def dot_first(a, b):
    return lax.dot_general(a, b, (((0,), (0,)), ((), ())), preferred_element_type=F32)


def place(rows, cols, shift):
    row = lax.broadcasted_iota(jnp.int32, (rows, cols), 0)
    col = lax.broadcasted_iota(jnp.int32, (rows, cols), 1)
    return jnp.where(col == row + shift, 1.0, 0.0).astype(F32).astype(BF16)


def kernel(
    n_kv,
    n_tp,
    res_ref,
    gain_first_ref,
    gain_mixer_ref,
    gain_second_ref,
    beta_ref,
    decay_ref,
    rate_ref,
    bias_ref,
    head_gain_ref,
    state_hbm,
    gate1_hbm,
    up1_hbm,
    down1_hbm,
    wq_hbm,
    wk_hbm,
    wv_hbm,
    wo_hbm,
    out_hbm,
    gate2_hbm,
    up2_hbm,
    down2_hbm,
    res_out_ref,
    state,
    gate1,
    up1,
    down1,
    wq,
    wk,
    wv,
    wo,
    wout,
    gate2,
    up2,
    down2,
    res_all,
    s1a,
    r1a,
    s1b,
    r1b,
    hid1,
    par1,
    sma,
    rma,
    smb,
    rmb,
    smc,
    rmc,
    nrm,
    parm,
    s2a,
    r2a,
    s2b,
    r2b,
    hid2,
    fin_send,
    fin_recv,
    qk_rows,
    val_rows,
    dec_rows,
    pred_rows,
    read_rows,
    w_sem,
    in_sem,
    send_sem,
    recv_sem,
):
    kv = lax.axis_index("kv")
    tp = lax.axis_index("tp")
    batch, piece = res_ref.shape
    depth = gate1.shape[0]
    width = depth * n_kv
    own_rows = batch // n_kv
    heads = state.shape[1]
    size = state.shape[2]
    key_cols = wq.shape[1]
    key_heads = key_cols // size
    repeat = heads // key_heads
    half = n_kv // 2
    groups = n_kv // GROUP

    turned = lax.rem(kv + GROUP - 2, GROUP)
    my_c = kv // GROUP
    my_s = turned // 4
    my_e = lax.rem(turned, 4) // 2
    my_b = lax.rem(turned, 2)
    my_j = my_c * 4 + my_e * 2 + my_b

    def device_at(c, stream, e, b):
        return c * GROUP + lax.rem(stream * 4 + e * 2 + b + 2, GROUP)

    def start_of(stream, j):
        return ((j // 4) * GROUP + (stream * 4 + j % 4 + 2) % GROUP) * own_rows

    def rows_of(value, stream):
        parts = [value[start_of(stream, j) : start_of(stream, j) + own_rows] for j in range(half)]
        return jnp.concatenate(parts, axis=0)

    weight_pairs = (
        (gate1_hbm, gate1),
        (up1_hbm, up1),
        (down1_hbm, down1),
        (wq_hbm, wq),
        (wk_hbm, wk),
        (wv_hbm, wv),
        (wo_hbm, wo),
        (out_hbm, wout),
        (gate2_hbm, gate2),
        (up2_hbm, up2),
        (down2_hbm, down2),
    )
    loads = [
        pltpu.make_async_copy(src, dst, w_sem.at[i]) for i, (src, dst) in enumerate(weight_pairs)
    ]
    for load in loads[:7]:
        load.start()

    barrier = pltpu.get_barrier_semaphore()
    for off in range(1, n_tp):
        pl.semaphore_signal(
            barrier,
            inc=1,
            device_id={"tp": lax.rem(tp + off, n_tp)},
            device_id_type=pl.DeviceIdType.MESH,
        )
    for off in range(1, n_kv):
        pl.semaphore_signal(
            barrier,
            inc=1,
            device_id={"kv": lax.rem(kv + off, n_kv)},
            device_id_type=pl.DeviceIdType.MESH,
        )
    with ns("barrier"):
        pl.semaphore_wait(barrier, n_tp - 1 + n_kv - 1)

    pending = []

    def remote(event, index, src, dst, axis, peer):
        return pltpu.make_async_remote_copy(
            src_ref=src,
            dst_ref=dst,
            send_sem=send_sem.at[event, index],
            recv_sem=recv_sem.at[event, index],
            device_id={axis: peer},
            device_id_type=pl.DeviceIdType.MESH,
        )

    def send_tp(event, src_of, dst_of):
        copies = []
        for off in range(1, n_tp):
            peer = lax.rem(tp + off, n_tp)
            copy = remote(event, off, src_of(off), dst_of(off), "tp", peer)
            copy.start()
            pending.append((copy, None))
            copies.append(copy)
        return copies

    steps = [(dc, de, db) for dc in range(groups) for de in (1, 0) for db in (1, 0)]

    def each_kv(stream, make):
        turn = lax.rem(stream + 2 - my_s, 2)
        for dc, de, db in steps:
            c, e, b = lax.rem(my_c + dc, groups), lax.rem(my_e + de, 2), lax.rem(my_b + db, 2)
            index = dc * GROUP + turn * 4 + de * 2 + db
            copy = make(index, device_at(c, stream, e, b), c * 4 + e * 2 + b)
            if (dc, de, db) == (0, 0, 0):
                pl.when(my_s != stream)(copy.start)
                pending.append((copy, stream))
            else:
                copy.start()
                pending.append((copy, None))

    def scatter(event, stream, sends, receives):
        each_kv(
            stream,
            lambda index, peer, j: remote(
                event, index, sends.at[stream, j], receives.at[index], "kv", peer
            ),
        )

    def collect(event, sends, receives):
        total = sends[my_s, my_j].astype(F32)
        for index in range(1, n_kv):
            remote(event, index, receives.at[index], receives.at[index], "kv", kv).wait_recv()
            total = total + receives[index].astype(F32)
        return total

    def spread(event, slots):
        own = slots.at[my_s, my_j]
        for stream in range(2):
            each_kv(stream, lambda index, peer, j: remote(event, index, own, own, "kv", peer))

    def arrive(event, stream, slots):
        turn = lax.rem(my_s + 2 - stream, 2)
        for dc, de, db in reversed(steps):
            index = dc * GROUP + turn * 4 + de * 2 + db
            copy = remote(event, index, slots.at[stream, 0], slots.at[stream, 0], "kv", kv)
            if (dc, de, db) == (0, 0, 0):
                pl.when(my_s != stream)(copy.wait_recv)
            else:
                copy.wait_recv()

    def put(ref, stream, offset, value):
        cols = value.shape[1]
        ref[stream, :, :, offset : offset + cols] = value.reshape(half, own_rows, cols).astype(BF16)

    def square_lanes(residual):
        squares = jnp.sum(residual * residual, axis=1, keepdims=True)
        high = squares.astype(BF16).astype(F32)
        lane = lax.broadcasted_iota(jnp.int32, (residual.shape[0], LANES), 1)
        return jnp.where(lane == 64, high, jnp.where(lane == 65, squares - high, 0.0))

    def row_scale(extra):
        squares = extra[:, 64:65] + extra[:, 65:66]
        return lax.rsqrt(squares / width + EPS)

    def flat(slots, stream):
        both = slots[stream].astype(F32)
        return both.reshape(half * own_rows, both.shape[2]).astype(BF16)

    def share(event, stream, value, slots):
        slots[stream, tp] = value.astype(BF16)
        own = slots.at[stream, tp]
        return send_tp(event, lambda off: own, lambda off: own)

    def join(copies, stream, slots):
        for copy in copies:
            copy.wait_recv()
        total = slots[stream, 0].astype(F32)
        for other in range(1, n_tp):
            total = total + slots[stream, other].astype(F32)
        return total

    def ffn_in(event, stream, residual, gain_ref, w_gate, w_up, bufs):
        send_a, recv_a, send_b, recv_b = bufs
        up_end = pad_lanes(w_gate.shape[1])
        scaled = (residual * gain_ref[...]).astype(BF16)
        put(send_a, stream, 0, dot(scaled, w_gate[...]))
        scatter(event, stream, send_a, recv_a)
        put(send_b, stream, 0, dot(scaled, w_up[...]))
        put(send_b, stream, up_end, square_lanes(residual))
        scatter(event + 1, stream, send_b, recv_b)

    def ffn_mid(event, bufs, hid):
        send_a, recv_a, send_b, recv_b = bufs
        hidden_cols = hid.shape[-1]
        up_end = pad_lanes(hidden_cols)
        with ns("f_rs_a"):
            gate_sum = collect(event, send_a, recv_a)[:, :hidden_cols]
        with ns("f_rs_b"):
            rest = collect(event + 1, send_b, recv_b)
        scale = row_scale(rest[:, up_end:])
        hidden = (silu(gate_sum * scale) * (rest[:, :hidden_cols] * scale)).astype(BF16)
        hid[my_s, my_j] = hidden
        spread(event + 2, hid)

    copies = send_tp(0, lambda off: res_ref, lambda off: res_all.at[tp])
    for load in loads[7:]:
        load.start()
    for row in range(own_rows):
        pltpu.make_async_copy(state_hbm.at[row], state.at[row], in_sem.at[row]).start()
    decay_exp = jnp.exp(rate_ref[...])
    extra_weight = (
        dot_first(beta_ref[...], place_heads(beta_ref.shape[0], tp * heads, 0, heads))
        + dot_first(decay_ref[...], place_heads(beta_ref.shape[0], tp * heads, heads, heads))
    ).astype(BF16)
    whole = dot(res_ref[...], place(piece, depth, tp * piece))
    with ns("tp_gather"):
        for off in range(1, n_tp):
            copies[off - 1].wait_recv()
            source = lax.rem(tp + n_tp - off, n_tp)
            whole = whole + dot(res_all[source], place(piece, depth, source * piece))

    first_bufs = (s1a, r1a, s1b, r1b)
    residual = [rows_of(whole, stream) for stream in range(2)]
    loads[0].wait()
    loads[1].wait()
    with ns("f1_in"):
        for stream in range(2):
            ffn_in(1, stream, residual[stream], gain_first_ref, gate1, up1, first_bufs)
    ffn_mid(1, first_bufs, hid1)
    loads[2].wait()
    shared = []
    for stream in range(2):
        with ns("f1_ag%d" % stream):
            arrive(3, stream, hid1)
        shared.append(share(4 + stream, stream, dot(flat(hid1, stream), down1[...]), par1))
    for load in loads[3:7]:
        load.wait()
    after_first = []
    for stream in range(2):
        with ns("exch1_%d" % stream):
            branch = join(shared[stream], stream, par1)
        kept = (residual[stream] + 0.5 * branch).astype(BF16).astype(F32)
        after_first.append(kept)
        scaled = (kept * gain_mixer_ref[...]).astype(BF16)
        with ns("m_in"):
            put(sma, stream, 0, dot(scaled, wq[...]))
            put(sma, stream, key_cols, dot(scaled, wk[...]))
            put(sma, stream, 2 * key_cols, dot(scaled, extra_weight) + square_lanes(kept))
            scatter(6, stream, sma, rma)
            put(smb, stream, 0, dot(scaled, wv[...]))
            scatter(7, stream, smb, rmb)
            put(smc, stream, 0, dot(scaled, wo[...]))
            scatter(8, stream, smc, rmc)

    with ns("m_rs_a"):
        keys_sum = collect(6, sma, rma)
    extra = keys_sum[:, 2 * key_cols :]
    scale = row_scale(extra)
    for head in range(key_heads):
        for slot, start, factor in (
            (head, head * size, size ** (-0.5)),
            (key_heads + head, key_cols + head * size, 1.0),
        ):
            act = silu(keys_sum[:, start : start + size] * scale)
            unit = act * lax.rsqrt(jnp.sum(act * act, axis=1, keepdims=True) + EPS)
            qk_rows[:, slot, :] = unit * factor
    gates = extra * scale
    beta_pre = gates[:, :heads]
    decay_pre = gates[:, heads : 2 * heads] + bias_ref[...]
    beta_gate = 1.0 / (1.0 + jnp.exp(-beta_pre))
    softplus = jnp.maximum(decay_pre, 0.0) + jnp.log1p(jnp.exp(-jnp.abs(decay_pre)))
    decay_gate = jnp.exp(-decay_exp * softplus)
    for head in range(heads):
        dec_rows[:, head, :] = jnp.broadcast_to(decay_gate[:, head : head + 1], (own_rows, size))

    def look(row, carry):
        pltpu.make_async_copy(state_hbm.at[row], state.at[row], in_sem.at[row]).wait()
        columns = qk_rows[row].T
        for head in range(heads):
            kh = head // repeat
            key_col = columns[:, key_heads + kh : key_heads + kh + 1]
            query_col = columns[:, kh : kh + 1]
            old = state[row, head]
            pred_rows[row, head : head + 1, :] = jnp.sum(old * key_col, axis=0, keepdims=True)
            read_rows[row, head : head + 1, :] = jnp.sum(old * query_col, axis=0, keepdims=True)
        return carry

    with ns("look"):
        lax.fori_loop(0, own_rows, look, 0)

    with ns("m_rs_b"):
        values = silu(collect(7, smb, rmb) * scale)
    with ns("m_rs_c"):
        out_gate = silu(collect(8, smc, rmc) * scale)
    with ns("m_norm"):
        for head in range(heads):
            kh = head // repeat
            cols = slice(head * size, (head + 1) * size)
            decay = decay_gate[:, head : head + 1]
            correction = beta_gate[:, head : head + 1] * (
                values[:, cols] - decay * pred_rows[:, head, :]
            )
            val_rows[:, head, :] = correction
            match = jnp.sum(
                qk_rows[:, kh, :] * qk_rows[:, key_heads + kh, :], axis=1, keepdims=True
            )
            reading = decay * read_rows[:, head, :] + match * correction
            mean = jnp.mean(reading * reading, axis=1, keepdims=True)
            normed = reading * lax.rsqrt(mean + EPS) * head_gain_ref[...]
            nrm[my_s, my_j, :, cols] = (normed * out_gate[:, cols]).astype(BF16)
        spread(9, nrm)

    loads[7].wait()
    shared = []
    for stream in range(2):
        with ns("m_ag%d" % stream):
            arrive(9, stream, nrm)
        shared.append(share(10 + stream, stream, dot(flat(nrm, stream), wout[...]), parm))

    second_bufs = (s2a, r2a, s2b, r2b)
    loads[8].wait()
    loads[9].wait()
    after_mixer = []
    for stream in range(2):
        with ns("exch2_%d" % stream):
            branch = join(shared[stream], stream, parm)
        kept = (after_first[stream] + branch).astype(BF16).astype(F32)
        after_mixer.append(kept)
        with ns("f2_in"):
            ffn_in(12, stream, kept, gain_second_ref, gate2, up2, second_bufs)

    def update(row, carry):
        columns = qk_rows[row].T
        row_dec, row_vals = dec_rows[row], val_rows[row]
        for head in range(heads):
            kh = head // repeat
            key_col = columns[:, key_heads + kh : key_heads + kh + 1]
            state[row, head] = (
                state[row, head] * row_dec[head : head + 1, :]
                + key_col * row_vals[head : head + 1, :]
            )
        return carry

    with ns("update"):
        lax.fori_loop(0, own_rows, update, 0)

    ffn_mid(12, second_bufs, hid2)
    loads[10].wait()
    finals = []
    mine = place_back(depth, piece, tp)
    for stream in range(2):
        with ns("f2_ag%d" % stream):
            arrive(14, stream, hid2)
        product = dot(flat(hid2, stream), down2[...]).astype(BF16)
        for off in range(1, n_tp):
            peer = lax.rem(tp + off, n_tp)
            fin_send[stream, off] = dot(product, place_back(depth, piece, peer)).astype(BF16)
        copies = send_tp(
            15 + stream,
            lambda off: fin_send.at[stream, off],
            lambda off: fin_recv.at[stream, off],
        )
        own_cols = dot(after_mixer[stream].astype(BF16), mine)
        finals.append((copies, own_cols, dot(product, mine)))
    for stream, (copies, own_cols, branch) in enumerate(finals):
        with ns("fin%d" % stream):
            for off in range(1, n_tp):
                copies[off - 1].wait_recv()
                branch = branch + fin_recv[stream, off].astype(F32)
        done = own_cols + 0.5 * branch
        for j in range(half):
            start = start_of(stream, j)
            res_out_ref[start : start + own_rows] = done[j * own_rows : (j + 1) * own_rows].astype(
                BF16
            )

    for copy, stream in pending:
        if stream is None:
            copy.wait_send()
        else:
            pl.when(my_s != stream)(copy.wait_send)


def place_back(rows, cols, peer):
    row = lax.broadcasted_iota(jnp.int32, (rows, cols), 0)
    col = lax.broadcasted_iota(jnp.int32, (rows, cols), 1)
    return jnp.where(row == col + peer * cols, 1.0, 0.0).astype(F32).astype(BF16)


def place_heads(rows, first, lane_start, count):
    row = lax.broadcasted_iota(jnp.int32, (rows, LANES), 0)
    col = lax.broadcasted_iota(jnp.int32, (rows, LANES), 1)
    inside = (col >= lane_start) & (col < lane_start + count)
    hit = inside & (row == col - lane_start + first)
    return jnp.where(hit, 1.0, 0.0).astype(F32).astype(BF16)


def body(
    n_kv,
    n_tp,
    residual_in,
    delta_state,
    norm_gain_first,
    gate_first,
    up_first,
    down_first,
    norm_gain_mixer,
    query_weight,
    key_weight,
    value_weight,
    output_gate_weight,
    beta_weight,
    decay_weight,
    decay_rate,
    decay_bias,
    head_gain,
    out_weight,
    norm_gain_second,
    gate_second,
    up_second,
    down_second,
):
    batch, piece = residual_in.shape
    depth, hidden = gate_first.shape
    own_rows, heads, size, _ = delta_state.shape
    key_cols = query_weight.shape[1]
    val_cols = value_weight.shape[1]
    key_heads = key_cols // size
    hp = pad_lanes(hidden)

    def like(x):
        return pltpu.VMEM(x.shape, x.dtype)

    def slots(cols):
        return pltpu.VMEM((n_kv, own_rows, cols), BF16)

    def split(cols):
        return pltpu.VMEM((2, n_kv // 2, own_rows, cols), BF16)

    def row_buf(count):
        return pltpu.VMEM((own_rows, count, size), F32)

    tp_slots = pltpu.VMEM((2, n_tp, batch // 2, depth), BF16)
    ffn_bufs = [split(hp), slots(hp), split(hp + LANES), slots(hp + LANES), split(hidden), tp_slots]
    wide = 2 * key_cols + LANES
    mixer_bufs = [
        split(wide),
        slots(wide),
        split(val_cols),
        slots(val_cols),
        split(val_cols),
        slots(val_cols),
        split(heads * size),
        tp_slots,
    ]
    big = (
        gate_first,
        up_first,
        down_first,
        query_weight,
        key_weight,
        value_weight,
        output_gate_weight,
        out_weight,
        gate_second,
        up_second,
        down_second,
    )
    small = (
        residual_in,
        norm_gain_first[None, :],
        norm_gain_mixer[None, :],
        norm_gain_second[None, :],
        beta_weight.T,
        decay_weight.T,
        decay_rate[None, :],
        decay_bias[None, :],
        head_gain[None, :],
    )
    vmem = pl.BlockSpec(memory_space=pltpu.VMEM)
    hbm = pl.BlockSpec(memory_space=pl.ANY)
    most = max(n_kv, n_tp)
    return pl.pallas_call(
        functools.partial(kernel, n_kv, n_tp),
        out_shape=(
            pltpu.VMEM(residual_in.shape, BF16),
            pltpu.VMEM(delta_state.shape, F32),
        ),
        in_specs=[vmem] * len(small) + [hbm] * (1 + len(big)),
        out_specs=(vmem, vmem),
        scratch_shapes=[like(x) for x in big]
        + [pltpu.VMEM((n_tp, batch, piece), BF16)]
        + ffn_bufs
        + mixer_bufs
        + ffn_bufs[:-1]
        + [pltpu.VMEM((2, n_tp, batch // 2, piece), BF16)] * 2
        + [row_buf(2 * key_heads), row_buf(heads), row_buf(heads), row_buf(heads), row_buf(heads)]
        + [
            pltpu.SemaphoreType.DMA((len(big),)),
            pltpu.SemaphoreType.DMA((own_rows,)),
            pltpu.SemaphoreType.DMA((17, most)),
            pltpu.SemaphoreType.DMA((17, most)),
        ],
        compiler_params=pltpu.CompilerParams(
            collective_id=0, has_side_effects=True, vmem_limit_bytes=58 * 1024 * 1024
        ),
        name="layer",
    )(*small, delta_state, *big)


def solution(mesh):
    placed = (
        P(None, ("kv", "tp")),
        P("kv", "tp", None, None),
        P("kv"),
        P("kv", "tp"),
        P("kv", "tp"),
        P("tp", "kv"),
        P("kv"),
        P("kv", "tp"),
        P("kv", "tp"),
        P("kv", "tp"),
        P("kv", "tp"),
        P("kv", None),
        P("kv", None),
        P("tp"),
        P("tp"),
        P(),
        P("tp", "kv"),
        P("kv"),
        P("kv", "tp"),
        P("kv", "tp"),
        P("tp", "kv"),
    )
    return jax.shard_map(
        functools.partial(body, mesh.shape["kv"], mesh.shape["tp"]),
        mesh=mesh,
        in_specs=placed,
        out_specs=(P(None, ("kv", "tp")), P("kv", "tp", None, None)),
        check_vma=False,
    )
```

time: 79.1 us -> 69.8 us (0.88)
  Pallas kernels: 72.2 us -> 66.3 us
  local copies, waits for them, and re-layouts: 6.02 us -> 2.62 us
    pallas_call x1, Pallas kernels: 72.2 us -> 66.3 us  [body(): pl.pallas_call(functools.partial(kernel, n_kv, n_tp), out_shape=(pltpu.VM...]
    unnamed x2, local copies, waits for them, and re-layouts: 6.02 us -> 2.62 us
where the time goes in v1:
time: 69.8 us; the launch traced here: 69.6 us
  Pallas kernels  66.3 us (95%)
  local copies, waits for them, and re-layouts  2.62 us (4%)
    pallas_call x1, Pallas kernels, body(): pl.pallas_call(functools.partial(kernel, n_kv, n_tp), out_shape=(pltpu.VM...  66.3 us
    unnamed x2, local copies, waits for them, and re-layouts  2.62 us

profile of v1, /device:TPU:0, one launch (start us, length us, event | category | flops | bytes accessed | tf_op | source)
XLA Modules:
  0.0 69.6 jit_solution(16253996667882737346)
XLA Ops:
  0.6 66.3 %layer.1 = (bf16[64,64]{1,0:T(8,128)(2,1)S(1)}, f32[8,8,128,128]{3,2,1,0:T(8,128)S(1)}) custom-call(bf16[64,64]{1,0:T(8,128)(2,1)} %res_ref.1, f32[1,256]{1,0:T(1,128)} %bitcast.10, f32[1,256]{1,0:T(1,128)} %bitcast.11, f32[1,256]{1,0:T(1,128)} %bitcast.12, bf16[32,256]{1,0:T(8,128)(2,1)} %bitcast.8, bf16[32,256]{1,0:T(8,128)(2,1)} %bitcast.9, ...), custom_call_target="tpu_custom_call" | custom-call | tf_op jit(solution)/shard_map/layer/pallas_call | solution.py:576
  67.0 0.6 copy.25
  67.6 2.0 %copy.26 = f32[8,8,128,128]{3,2,1,0:T(8,128)} copy(f32[8,8,128,128]{3,2,1,0:T(8,128)S(1)} %get-tuple-element.3) | data formatting | bytes 8388608

commit v2 on v1

--- a/solution.py
+++ b/solution.py
@@ -9,6 +9,7 @@
 
 EPS = 1e-06
 GROUP = 8
+UNROLL = 8
 LANES = 128
 BF16 = jnp.bfloat16
 F32 = jnp.float32
@@ -40,15 +41,15 @@
 def kernel(
     n_kv,
     n_tp,
-    res_ref,
-    gain_first_ref,
-    gain_mixer_ref,
-    gain_second_ref,
-    beta_ref,
-    decay_ref,
-    rate_ref,
-    bias_ref,
-    head_gain_ref,
+    res_hbm,
+    gain_first_hbm,
+    gain_mixer_hbm,
+    gain_second_hbm,
+    beta_hbm,
+    decay_hbm,
+    rate_hbm,
+    bias_hbm,
+    head_gain_hbm,
     state_hbm,
     gate1_hbm,
     up1_hbm,
@@ -63,6 +64,15 @@
     down2_hbm,
     res_out_ref,
     state,
+    res_ref,
+    gain_first_ref,
+    gain_mixer_ref,
+    gain_second_ref,
+    beta_ref,
+    decay_ref,
+    rate_ref,
+    bias_ref,
+    head_gain_ref,
     gate1,
     up1,
     down1,
@@ -102,9 +112,11 @@
     pred_rows,
     read_rows,
     w_sem,
+    small_sem,
     in_sem,
     send_sem,
     recv_sem,
+    late_sem,
 ):
     kv = lax.axis_index("kv")
     tp = lax.axis_index("tp")
@@ -125,7 +137,9 @@
     my_s = turned // 4
     my_e = lax.rem(turned, 4) // 2
     my_b = lax.rem(turned, 2)
-    my_j = my_c * 4 + my_e * 2 + my_b
+    my_i = my_c * 4 + my_e * 2 + my_b
+    my_j = my_s * half + my_i
+    owner = my_s == 0
 
     def device_at(c, stream, e, b):
         return c * GROUP + lax.rem(stream * 4 + e * 2 + b + 2, GROUP)
@@ -153,9 +167,22 @@
     loads = [
         pltpu.make_async_copy(src, dst, w_sem.at[i]) for i, (src, dst) in enumerate(weight_pairs)
     ]
-    for load in loads[:7]:
-        load.start()
-
+    small_pairs = (
+        (res_hbm, res_ref),
+        (gain_first_hbm, gain_first_ref),
+        (gain_mixer_hbm, gain_mixer_ref),
+        (gain_second_hbm, gain_second_ref),
+        (beta_hbm, beta_ref),
+        (decay_hbm, decay_ref),
+        (rate_hbm, rate_ref),
+        (bias_hbm, bias_ref),
+        (head_gain_hbm, head_gain_ref),
+    )
+    smalls = [
+        pltpu.make_async_copy(src, dst, small_sem.at[i])
+        for i, (src, dst) in enumerate(small_pairs)
+    ]
+    smalls[0].start()
     barrier = pltpu.get_barrier_semaphore()
     for off in range(1, n_tp):
         pl.semaphore_signal(
@@ -171,79 +198,103 @@
             device_id={"kv": lax.rem(kv + off, n_kv)},
             device_id_type=pl.DeviceIdType.MESH,
         )
+    for copy in smalls[1:] + loads[:3]:
+        copy.start()
     with ns("barrier"):
         pl.semaphore_wait(barrier, n_tp - 1 + n_kv - 1)
 
-    pending = []
-
-    def remote(event, index, src, dst, axis, peer):
+    def remote(src, dst, axis, peer, left, landed):
         return pltpu.make_async_remote_copy(
             src_ref=src,
             dst_ref=dst,
-            send_sem=send_sem.at[event, index],
-            recv_sem=recv_sem.at[event, index],
+            send_sem=left,
+            recv_sem=landed,
             device_id={axis: peer},
             device_id_type=pl.DeviceIdType.MESH,
         )
 
-    def send_tp(event, src_of, dst_of):
-        copies = []
+    sent = []
+
+    def send_tp(event, src_of, dst_of, block):
+        sems = send_sem.at[event], recv_sem.at[event]
         for off in range(1, n_tp):
             peer = lax.rem(tp + off, n_tp)
-            copy = remote(event, off, src_of(off), dst_of(off), "tp", peer)
-            copy.start()
-            pending.append((copy, None))
-            copies.append(copy)
-        return copies
-
-    steps = [(dc, de, db) for dc in range(groups) for de in (1, 0) for db in (1, 0)]
+            remote(src_of(off), dst_of(off), "tp", peer, *sems).start()
+        every = remote(block, block, "tp", tp, *sems)
+        sent.append((None, every))
+        return every
+
+    steps = [
+        (dc, de, db) for dc in range(groups - 1, -1, -1) for de in (1, 0) for db in (1, 0)
+    ]
 
     def each_kv(stream, make):
         turn = lax.rem(stream + 2 - my_s, 2)
         for dc, de, db in steps:
             c, e, b = lax.rem(my_c + dc, groups), lax.rem(my_e + de, 2), lax.rem(my_b + db, 2)
-            index = dc * GROUP + turn * 4 + de * 2 + db
-            copy = make(index, device_at(c, stream, e, b), c * 4 + e * 2 + b)
-            if (dc, de, db) == (0, 0, 0):
+            last = dc == 0 and de == 0 and db == 0
+            copy = make(
+                dc * GROUP + turn * 4 + de * 2 + db,
+                device_at(c, stream, e, b),
+                c * 4 + e * 2 + b,
+                last,
+            )
+            if last:
                 pl.when(my_s != stream)(copy.start)
-                pending.append((copy, stream))
             else:
                 copy.start()
-                pending.append((copy, None))
 
     def scatter(event, stream, sends, receives):
+        sems = send_sem.at[event], recv_sem.at[event]
         each_kv(
             stream,
-            lambda index, peer, j: remote(
-                event, index, sends.at[stream, j], receives.at[index], "kv", peer
+            lambda index, peer, j, last: remote(
+                sends.at[stream * half + j], receives.at[index], "kv", peer, *sems
             ),
         )
 
     def collect(event, sends, receives):
-        total = sends[my_s, my_j].astype(F32)
+        block = receives.at[pl.ds(1, n_kv - 1)]
+        every = remote(block, block, "kv", kv, send_sem.at[event], recv_sem.at[event])
+        every.wait_recv()
+        sent.append((None, every))
+        total = sends[my_j].astype(F32)
         for index in range(1, n_kv):
-            remote(event, index, receives.at[index], receives.at[index], "kv", kv).wait_recv()
             total = total + receives[index].astype(F32)
         return total
 
-    def spread(event, slots):
-        own = slots.at[my_s, my_j]
+    def spread(event, late, slots):
+        own = slots.at[my_j]
+        left = send_sem.at[event]
         for stream in range(2):
-            each_kv(stream, lambda index, peer, j: remote(event, index, own, own, "kv", peer))
-
-    def arrive(event, stream, slots):
-        turn = lax.rem(my_s + 2 - stream, 2)
-        for dc, de, db in reversed(steps):
-            index = dc * GROUP + turn * 4 + de * 2 + db
-            copy = remote(event, index, slots.at[stream, 0], slots.at[stream, 0], "kv", kv)
-            if (dc, de, db) == (0, 0, 0):
-                pl.when(my_s != stream)(copy.wait_recv)
-            else:
-                copy.wait_recv()
+            each_kv(
+                stream,
+                lambda index, peer, j, last: remote(
+                    own,
+                    own,
+                    "kv",
+                    peer,
+                    left,
+                    late_sem.at[late + my_s] if last else recv_sem.at[event + my_s],
+                ),
+            )
+        block = slots.at[pl.ds(0, n_kv - 1)]
+        sent.append((None, remote(block, block, "kv", kv, left, recv_sem.at[event])))
+
+    def arrive(event, late, stream, slots):
+        left = send_sem.at[event]
+        block = slots.at[pl.ds(0, half - 1)]
+        remote(block, block, "kv", kv, left, recv_sem.at[event + stream]).wait_recv()
+        own = slots.at[0]
+        pl.when(my_s != stream)(
+            remote(own, own, "kv", kv, left, late_sem.at[late + stream]).wait_recv
+        )
 
     def put(ref, stream, offset, value):
         cols = value.shape[1]
-        ref[stream, :, :, offset : offset + cols] = value.reshape(half, own_rows, cols).astype(BF16)
+        ref[stream * half : (stream + 1) * half, :, offset : offset + cols] = value.reshape(
+            half, own_rows, cols
+        ).astype(BF16)
 
     def square_lanes(residual):
         squares = jnp.sum(residual * residual, axis=1, keepdims=True)
@@ -256,20 +307,37 @@
         return lax.rsqrt(squares / width + EPS)
 
     def flat(slots, stream):
-        both = slots[stream].astype(F32)
+        both = slots[stream * half : (stream + 1) * half].astype(F32)
         return both.reshape(half * own_rows, both.shape[2]).astype(BF16)
 
     def share(event, stream, value, slots):
         slots[stream, tp] = value.astype(BF16)
         own = slots.at[stream, tp]
-        return send_tp(event, lambda off: own, lambda off: own)
-
-    def join(copies, stream, slots):
-        for copy in copies:
-            copy.wait_recv()
+        block = slots.at[stream, pl.ds(0, n_tp - 1)]
+        return send_tp(event, lambda off: own, lambda off: own, block)
+
+    def join(every, stream, slots):
+        every.wait_recv()
         total = slots[stream, 0].astype(F32)
         for other in range(1, n_tp):
             total = total + slots[stream, other].astype(F32)
+        return total
+
+    def to_owners(event, stream, sends, receives):
+        sems = send_sem.at[event], recv_sem.at[event + stream]
+        each_kv(
+            0,
+            lambda index, peer, j, last: remote(
+                sends.at[stream * half + j], receives.at[stream * n_kv + index], "kv", peer, *sems
+            ),
+        )
+
+    def owned(event, stream, sends, receives):
+        block = receives.at[pl.ds(stream * n_kv + 1, n_kv - 1)]
+        remote(block, block, "kv", kv, send_sem.at[event], recv_sem.at[event + stream]).wait_recv()
+        total = sends[stream * half + my_i].astype(F32)
+        for index in range(1, n_kv):
+            total = total + receives[stream * n_kv + index].astype(F32)
         return total
 
     def ffn_in(event, stream, residual, gain_ref, w_gate, w_up, bufs):
@@ -277,29 +345,65 @@
         up_end = pad_lanes(w_gate.shape[1])
         scaled = (residual * gain_ref[...]).astype(BF16)
         put(send_a, stream, 0, dot(scaled, w_gate[...]))
-        scatter(event, stream, send_a, recv_a)
+        to_owners(event, stream, send_a, recv_a)
         put(send_b, stream, 0, dot(scaled, w_up[...]))
         put(send_b, stream, up_end, square_lanes(residual))
-        scatter(event + 1, stream, send_b, recv_b)
-
-    def ffn_mid(event, bufs, hid):
+        to_owners(event + 2, stream, send_b, recv_b)
+
+    def ffn_mid(event, late, stream, bufs, hid):
         send_a, recv_a, send_b, recv_b = bufs
         hidden_cols = hid.shape[-1]
         up_end = pad_lanes(hidden_cols)
         with ns("f_rs_a"):
-            gate_sum = collect(event, send_a, recv_a)[:, :hidden_cols]
+            gate_sum = owned(event, stream, send_a, recv_a)[:, :hidden_cols]
         with ns("f_rs_b"):
-            rest = collect(event + 1, send_b, recv_b)
+            rest = owned(event + 2, stream, send_b, recv_b)
         scale = row_scale(rest[:, up_end:])
         hidden = (silu(gate_sum * scale) * (rest[:, :hidden_cols] * scale)).astype(BF16)
-        hid[my_s, my_j] = hidden
-        spread(event + 2, hid)
-
-    copies = send_tp(0, lambda off: res_ref, lambda off: res_all.at[tp])
-    for load in loads[7:]:
+        hid[stream * half + my_i] = hidden
+        own = hid.at[stream * half + my_i]
+        left = send_sem.at[event + 4 + stream]
+        for target in range(2):
+            for dc, de, db in steps:
+                last = dc == 0 and de == 0 and db == 0
+                if not (last and target == 0):
+                    c, e, b = (
+                        lax.rem(my_c + dc, groups),
+                        lax.rem(my_e + de, 2),
+                        lax.rem(my_b + db, 2),
+                    )
+                    landed = late_sem.at[late + stream] if last else recv_sem.at[event + 4 + stream]
+                    remote(own, own, "kv", device_at(c, target, e, b), left, landed).start()
+
+    def ffn_sent(event, bufs, hid):
+        for buf, at in ((bufs[1], event), (bufs[3], event + 2)):
+            for cond, count in ((owner, n_kv - 2), (jnp.logical_not(owner), n_kv)):
+                block = buf.at[pl.ds(0, count)]
+                sent.append(
+                    (cond, remote(block, block, "kv", kv, send_sem.at[at], recv_sem.at[at]))
+                )
+        for stream in range(2):
+            block = hid.at[pl.ds(0, n_kv - 1)]
+            at = event + 4 + stream
+            sent.append((owner, remote(block, block, "kv", kv, send_sem.at[at], recv_sem.at[at])))
+
+    def ffn_arrive(event, late, stream, hid):
+        at = event + 4 + stream
+        block = hid.at[pl.ds(0, half - 1)]
+        remote(block, block, "kv", kv, send_sem.at[at], recv_sem.at[at]).wait_recv()
+        own = hid.at[0]
+        pl.when(jnp.logical_not(owner))(
+            remote(own, own, "kv", kv, send_sem.at[at], late_sem.at[late + stream]).wait_recv
+        )
+
+    smalls[0].wait()
+    every = send_tp(0, lambda off: res_ref, lambda off: res_all.at[tp], res_all.at[pl.ds(0, n_tp - 1)])
+    for load in loads[3:]:
         load.start()
-    for row in range(own_rows):
-        pltpu.make_async_copy(state_hbm.at[row], state.at[row], in_sem.at[row]).start()
+    state_load = pltpu.make_async_copy(state_hbm, state, in_sem)
+    state_load.start()
+    for copy in smalls[1:]:
+        copy.wait()
     decay_exp = jnp.exp(rate_ref[...])
     extra_weight = (
         dot_first(beta_ref[...], place_heads(beta_ref.shape[0], tp * heads, 0, heads))
@@ -307,8 +411,8 @@
     ).astype(BF16)
     whole = dot(res_ref[...], place(piece, depth, tp * piece))
     with ns("tp_gather"):
+        every.wait_recv()
         for off in range(1, n_tp):
-            copies[off - 1].wait_recv()
             source = lax.rem(tp + n_tp - off, n_tp)
             whole = whole + dot(res_all[source], place(piece, depth, source * piece))
 
@@ -319,13 +423,15 @@
     with ns("f1_in"):
         for stream in range(2):
             ffn_in(1, stream, residual[stream], gain_first_ref, gate1, up1, first_bufs)
-    ffn_mid(1, first_bufs, hid1)
+    for stream in range(2):
+        pl.when(owner)(functools.partial(ffn_mid, 1, 0, stream, first_bufs, hid1))
+    ffn_sent(1, first_bufs, hid1)
     loads[2].wait()
     shared = []
     for stream in range(2):
         with ns("f1_ag%d" % stream):
-            arrive(3, stream, hid1)
-        shared.append(share(4 + stream, stream, dot(flat(hid1, stream), down1[...]), par1))
+            ffn_arrive(1, 0, stream, hid1)
+        shared.append(share(7 + stream, stream, dot(flat(hid1, stream), down1[...]), par1))
     for load in loads[3:7]:
         load.wait()
     after_first = []
@@ -339,14 +445,14 @@
             put(sma, stream, 0, dot(scaled, wq[...]))
             put(sma, stream, key_cols, dot(scaled, wk[...]))
             put(sma, stream, 2 * key_cols, dot(scaled, extra_weight) + square_lanes(kept))
-            scatter(6, stream, sma, rma)
+            scatter(9, stream, sma, rma)
             put(smb, stream, 0, dot(scaled, wv[...]))
-            scatter(7, stream, smb, rmb)
+            scatter(10, stream, smb, rmb)
             put(smc, stream, 0, dot(scaled, wo[...]))
-            scatter(8, stream, smc, rmc)
+            scatter(11, stream, smc, rmc)
 
     with ns("m_rs_a"):
-        keys_sum = collect(6, sma, rma)
+        keys_sum = collect(9, sma, rma)
     extra = keys_sum[:, 2 * key_cols :]
     scale = row_scale(extra)
     for head in range(key_heads):
@@ -367,7 +473,6 @@
         dec_rows[:, head, :] = jnp.broadcast_to(decay_gate[:, head : head + 1], (own_rows, size))
 
     def look(row, carry):
-        pltpu.make_async_copy(state_hbm.at[row], state.at[row], in_sem.at[row]).wait()
         columns = qk_rows[row].T
         for head in range(heads):
             kh = head // repeat
@@ -379,12 +484,13 @@
         return carry
 
     with ns("look"):
-        lax.fori_loop(0, own_rows, look, 0)
+        state_load.wait()
+        lax.fori_loop(0, own_rows, look, 0, unroll=UNROLL)
 
     with ns("m_rs_b"):
-        values = silu(collect(7, smb, rmb) * scale)
+        values = silu(collect(10, smb, rmb) * scale)
     with ns("m_rs_c"):
-        out_gate = silu(collect(8, smc, rmc) * scale)
+        out_gate = silu(collect(11, smc, rmc) * scale)
     with ns("m_norm"):
         for head in range(heads):
             kh = head // repeat
@@ -400,15 +506,15 @@
             reading = decay * read_rows[:, head, :] + match * correction
             mean = jnp.mean(reading * reading, axis=1, keepdims=True)
             normed = reading * lax.rsqrt(mean + EPS) * head_gain_ref[...]
-            nrm[my_s, my_j, :, cols] = (normed * out_gate[:, cols]).astype(BF16)
-        spread(9, nrm)
+            nrm[my_j, :, cols] = (normed * out_gate[:, cols]).astype(BF16)
+        spread(12, 2, nrm)
 
     loads[7].wait()
     shared = []
     for stream in range(2):
         with ns("m_ag%d" % stream):
-            arrive(9, stream, nrm)
-        shared.append(share(10 + stream, stream, dot(flat(nrm, stream), wout[...]), parm))
+            arrive(12, 2, stream, nrm)
+        shared.append(share(14 + stream, stream, dot(flat(nrm, stream), wout[...]), parm))
 
     second_bufs = (s2a, r2a, s2b, r2b)
     loads[8].wait()
@@ -420,7 +526,7 @@
         kept = (after_first[stream] + branch).astype(BF16).astype(F32)
         after_mixer.append(kept)
         with ns("f2_in"):
-            ffn_in(12, stream, kept, gain_second_ref, gate2, up2, second_bufs)
+            ffn_in(16, stream, kept, gain_second_ref, gate2, up2, second_bufs)
 
     def update(row, carry):
         columns = qk_rows[row].T
@@ -434,31 +540,34 @@
             )
         return carry
 
-    with ns("update"):
-        lax.fori_loop(0, own_rows, update, 0)
-
-    ffn_mid(12, second_bufs, hid2)
+    for stream in range(2):
+        pl.when(owner)(functools.partial(ffn_mid, 16, 4, stream, second_bufs, hid2))
+    ffn_sent(16, second_bufs, hid2)
     loads[10].wait()
     finals = []
     mine = place_back(depth, piece, tp)
     for stream in range(2):
         with ns("f2_ag%d" % stream):
-            arrive(14, stream, hid2)
+            ffn_arrive(16, 4, stream, hid2)
         product = dot(flat(hid2, stream), down2[...]).astype(BF16)
         for off in range(1, n_tp):
             peer = lax.rem(tp + off, n_tp)
             fin_send[stream, off] = dot(product, place_back(depth, piece, peer)).astype(BF16)
-        copies = send_tp(
-            15 + stream,
+        every = send_tp(
+            22 + stream,
             lambda off: fin_send.at[stream, off],
             lambda off: fin_recv.at[stream, off],
+            fin_recv.at[stream, pl.ds(1, n_tp - 1)],
         )
         own_cols = dot(after_mixer[stream].astype(BF16), mine)
-        finals.append((copies, own_cols, dot(product, mine)))
-    for stream, (copies, own_cols, branch) in enumerate(finals):
+        finals.append((every, own_cols, dot(product, mine)))
+    with ns("update"):
+        lax.fori_loop(0, own_rows, update, 0, unroll=UNROLL)
+
+    for stream, (every, own_cols, branch) in enumerate(finals):
         with ns("fin%d" % stream):
+            every.wait_recv()
             for off in range(1, n_tp):
-                copies[off - 1].wait_recv()
                 branch = branch + fin_recv[stream, off].astype(F32)
         done = own_cols + 0.5 * branch
         for j in range(half):
@@ -467,11 +576,11 @@
                 BF16
             )
 
-    for copy, stream in pending:
-        if stream is None:
-            copy.wait_send()
+    for cond, every in sent:
+        if cond is None:
+            every.wait_send()
         else:
-            pl.when(my_s != stream)(copy.wait_send)
+            pl.when(cond)(every.wait_send)
 
 
 def place_back(rows, cols, peer):
@@ -524,26 +633,31 @@
     def like(x):
         return pltpu.VMEM(x.shape, x.dtype)
 
-    def slots(cols):
-        return pltpu.VMEM((n_kv, own_rows, cols), BF16)
-
-    def split(cols):
-        return pltpu.VMEM((2, n_kv // 2, own_rows, cols), BF16)
+    def slots(cols, times=1):
+        return pltpu.VMEM((times * n_kv, own_rows, cols), BF16)
+
 
     def row_buf(count):
         return pltpu.VMEM((own_rows, count, size), F32)
 
     tp_slots = pltpu.VMEM((2, n_tp, batch // 2, depth), BF16)
-    ffn_bufs = [split(hp), slots(hp), split(hp + LANES), slots(hp + LANES), split(hidden), tp_slots]
+    ffn_bufs = [
+        slots(hp),
+        slots(hp, 2),
+        slots(hp + LANES),
+        slots(hp + LANES, 2),
+        slots(hidden),
+        tp_slots,
+    ]
     wide = 2 * key_cols + LANES
     mixer_bufs = [
-        split(wide),
         slots(wide),
-        split(val_cols),
+        slots(wide),
         slots(val_cols),
-        split(val_cols),
         slots(val_cols),
-        split(heads * size),
+        slots(val_cols),
+        slots(val_cols),
+        slots(heads * size),
         tp_slots,
     ]
     big = (
@@ -572,16 +686,15 @@
     )
     vmem = pl.BlockSpec(memory_space=pltpu.VMEM)
     hbm = pl.BlockSpec(memory_space=pl.ANY)
-    most = max(n_kv, n_tp)
     return pl.pallas_call(
         functools.partial(kernel, n_kv, n_tp),
         out_shape=(
             pltpu.VMEM(residual_in.shape, BF16),
             pltpu.VMEM(delta_state.shape, F32),
         ),
-        in_specs=[vmem] * len(small) + [hbm] * (1 + len(big)),
+        in_specs=[hbm] * (len(small) + 1 + len(big)),
         out_specs=(vmem, vmem),
-        scratch_shapes=[like(x) for x in big]
+        scratch_shapes=[like(x) for x in (*small, *big)]
         + [pltpu.VMEM((n_tp, batch, piece), BF16)]
         + ffn_bufs
         + mixer_bufs
@@ -590,9 +703,11 @@
         + [row_buf(2 * key_heads), row_buf(heads), row_buf(heads), row_buf(heads), row_buf(heads)]
         + [
             pltpu.SemaphoreType.DMA((len(big),)),
-            pltpu.SemaphoreType.DMA((own_rows,)),
-            pltpu.SemaphoreType.DMA((17, most)),
-            pltpu.SemaphoreType.DMA((17, most)),
+            pltpu.SemaphoreType.DMA((len(small),)),
+            pltpu.SemaphoreType.DMA,
+            pltpu.SemaphoreType.DMA((24,)),
+            pltpu.SemaphoreType.DMA((24,)),
+            pltpu.SemaphoreType.DMA((6,)),
         ],
         compiler_params=pltpu.CompilerParams(
             collective_id=0, has_side_effects=True, vmem_limit_bytes=58 * 1024 * 1024

time: 69.8 us -> 62.7 us (0.90)
  Pallas kernels: 66.3 us -> 59.3 us
    pallas_call x1, Pallas kernels: 66.3 us -> 59.3 us  [body(): pl.pallas_call(functools.partial(kernel, n_kv, n_tp), out_shape=(pltpu.VM...]
where the time goes in v2:
time: 62.7 us; the launch traced here: 62.5 us
  Pallas kernels  59.3 us (95%)
  local copies, waits for them, and re-layouts  2.62 us (4%)
  between operations  0.65 us (1%)
    pallas_call x1, Pallas kernels, body(): pl.pallas_call(functools.partial(kernel, n_kv, n_tp), out_shape=(pltpu.VM...  59.3 us
    unnamed x2, local copies, waits for them, and re-layouts  2.62 us

profile of v2, /device:TPU:0, one launch (start us, length us, event | category | flops | bytes accessed | tf_op | source)
XLA Modules:
  0.0 62.5 jit_solution(9191936856466274737)
XLA Ops:
  0.6 59.3 %layer.1 = (bf16[64,64]{1,0:T(8,128)(2,1)S(1)}, f32[8,8,128,128]{3,2,1,0:T(8,128)S(1)}) custom-call(bf16[64,64]{1,0:T(8,128)(2,1)} %res_hbm.1, f32[1,256]{1,0:T(1,128)} %bitcast.10, f32[1,256]{1,0:T(1,128)} %bitcast.11, f32[1,256]{1,0:T(1,128)} %bitcast.12, bf16[32,256]{1,0:T(8,128)(2,1)} %bitcast.8, bf16[32,256]{1,0:T(8,128)(2,1)} %bitcast.9, ...), custom_call_target="tpu_custom_call" | custom-call | tf_op jit(solution)/shard_map/layer/pallas_call | solution.py:689
  59.9 0.6 copy.25
  60.5 2.0 %copy.26 = f32[8,8,128,128]{3,2,1,0:T(8,128)} copy(f32[8,8,128,128]{3,2,1,0:T(8,128)S(1)} %get-tuple-element.3) | data formatting | bytes 8388608

commit v3 on v2

--- a/solution.py
+++ b/solution.py
@@ -10,6 +10,7 @@
 EPS = 1e-06
 GROUP = 8
 UNROLL = 8
+ORDER = (0, 1)
 LANES = 128
 BF16 = jnp.bfloat16
 F32 = jnp.float32
@@ -191,17 +192,21 @@
             device_id={"tp": lax.rem(tp + off, n_tp)},
             device_id_type=pl.DeviceIdType.MESH,
         )
-    for off in range(1, n_kv):
-        pl.semaphore_signal(
-            barrier,
-            inc=1,
-            device_id={"kv": lax.rem(kv + off, n_kv)},
-            device_id_type=pl.DeviceIdType.MESH,
-        )
+
+    @pl.when(owner)
+    def greet():
+        for off in range(1, n_kv):
+            pl.semaphore_signal(
+                barrier,
+                inc=1,
+                device_id={"kv": lax.rem(kv + off, n_kv)},
+                device_id_type=pl.DeviceIdType.MESH,
+            )
+
     for copy in smalls[1:] + loads[:3]:
         copy.start()
     with ns("barrier"):
-        pl.semaphore_wait(barrier, n_tp - 1 + n_kv - 1)
+        pl.semaphore_wait(barrier, n_tp - 1 + half - 1 + my_s)
 
     def remote(src, dst, axis, peer, left, landed):
         return pltpu.make_async_remote_copy(
@@ -225,16 +230,18 @@
         return every
 
     steps = [
-        (dc, de, db) for dc in range(groups - 1, -1, -1) for de in (1, 0) for db in (1, 0)
+        (dc, dh, db) for dc in range(groups - 1, -1, -1) for dh in (1, 0) for db in (1, 0)
     ]
+    my_h = lax.rem(my_e + my_s, 2)
 
     def each_kv(stream, make):
         turn = lax.rem(stream + 2 - my_s, 2)
-        for dc, de, db in steps:
-            c, e, b = lax.rem(my_c + dc, groups), lax.rem(my_e + de, 2), lax.rem(my_b + db, 2)
-            last = dc == 0 and de == 0 and db == 0
+        for dc, dh, db in steps:
+            c, b = lax.rem(my_c + dc, groups), lax.rem(my_b + db, 2)
+            e = lax.rem(my_h + dh + stream, 2)
+            last = dc == 0 and dh == 0 and db == 0
             copy = make(
-                dc * GROUP + turn * 4 + de * 2 + db,
+                dc * GROUP + turn * 4 + dh * 2 + db,
                 device_at(c, stream, e, b),
                 c * 4 + e * 2 + b,
                 last,
@@ -364,12 +371,12 @@
         own = hid.at[stream * half + my_i]
         left = send_sem.at[event + 4 + stream]
         for target in range(2):
-            for dc, de, db in steps:
-                last = dc == 0 and de == 0 and db == 0
+            for dc, dh, db in steps:
+                last = dc == 0 and dh == 0 and db == 0
                 if not (last and target == 0):
                     c, e, b = (
                         lax.rem(my_c + dc, groups),
-                        lax.rem(my_e + de, 2),
+                        lax.rem(my_h + dh + target, 2),
                         lax.rem(my_b + db, 2),
                     )
                     landed = late_sem.at[late + stream] if last else recv_sem.at[event + 4 + stream]
@@ -421,25 +428,23 @@
     loads[0].wait()
     loads[1].wait()
     with ns("f1_in"):
-        for stream in range(2):
+        for stream in ORDER:
             ffn_in(1, stream, residual[stream], gain_first_ref, gate1, up1, first_bufs)
-    for stream in range(2):
+    for stream in ORDER:
         pl.when(owner)(functools.partial(ffn_mid, 1, 0, stream, first_bufs, hid1))
     ffn_sent(1, first_bufs, hid1)
-    loads[2].wait()
-    shared = []
-    for stream in range(2):
+    def first_out(stream):
         with ns("f1_ag%d" % stream):
             ffn_arrive(1, 0, stream, hid1)
-        shared.append(share(7 + stream, stream, dot(flat(hid1, stream), down1[...]), par1))
-    for load in loads[3:7]:
-        load.wait()
-    after_first = []
-    for stream in range(2):
+        return share(7 + stream, stream, dot(flat(hid1, stream), down1[...]), par1)
+
+    after_first = [None, None]
+
+    def mixer_in(stream, shared):
         with ns("exch1_%d" % stream):
-            branch = join(shared[stream], stream, par1)
+            branch = join(shared, stream, par1)
         kept = (residual[stream] + 0.5 * branch).astype(BF16).astype(F32)
-        after_first.append(kept)
+        after_first[stream] = kept
         scaled = (kept * gain_mixer_ref[...]).astype(BF16)
         with ns("m_in"):
             put(sma, stream, 0, dot(scaled, wq[...]))
@@ -450,6 +455,13 @@
             scatter(10, stream, smb, rmb)
             put(smc, stream, 0, dot(scaled, wo[...]))
             scatter(11, stream, smc, rmc)
+
+    for load in loads[2:7]:
+        load.wait()
+    shared = first_out(ORDER[0])
+    later = first_out(ORDER[1])
+    mixer_in(ORDER[0], shared)
+    mixer_in(ORDER[1], later)
 
     with ns("m_rs_a"):
         keys_sum = collect(9, sma, rma)
@@ -509,24 +521,27 @@
             nrm[my_j, :, cols] = (normed * out_gate[:, cols]).astype(BF16)
         spread(12, 2, nrm)
 
-    loads[7].wait()
-    shared = []
-    for stream in range(2):
+    def mixer_out(stream):
         with ns("m_ag%d" % stream):
             arrive(12, 2, stream, nrm)
-        shared.append(share(14 + stream, stream, dot(flat(nrm, stream), wout[...]), parm))
+        return share(14 + stream, stream, dot(flat(nrm, stream), wout[...]), parm)
 
     second_bufs = (s2a, r2a, s2b, r2b)
-    loads[8].wait()
-    loads[9].wait()
-    after_mixer = []
-    for stream in range(2):
+    after_mixer = [None, None]
+
+    def second_in(stream, shared):
         with ns("exch2_%d" % stream):
-            branch = join(shared[stream], stream, parm)
+            branch = join(shared, stream, parm)
         kept = (after_first[stream] + branch).astype(BF16).astype(F32)
-        after_mixer.append(kept)
+        after_mixer[stream] = kept
         with ns("f2_in"):
             ffn_in(16, stream, kept, gain_second_ref, gate2, up2, second_bufs)
+
+    for load in loads[7:10]:
+        load.wait()
+    shared = mixer_out(ORDER[0])
+    second_in(ORDER[0], shared)
+    second_in(ORDER[1], mixer_out(ORDER[1]))
 
     def update(row, carry):
         columns = qk_rows[row].T
@@ -540,13 +555,13 @@
             )
         return carry
 
-    for stream in range(2):
+    for stream in ORDER:
         pl.when(owner)(functools.partial(ffn_mid, 16, 4, stream, second_bufs, hid2))
     ffn_sent(16, second_bufs, hid2)
     loads[10].wait()
     finals = []
     mine = place_back(depth, piece, tp)
-    for stream in range(2):
+    for stream in ORDER:
         with ns("f2_ag%d" % stream):
             ffn_arrive(16, 4, stream, hid2)
         product = dot(flat(hid2, stream), down2[...]).astype(BF16)
@@ -560,11 +575,11 @@
             fin_recv.at[stream, pl.ds(1, n_tp - 1)],
         )
         own_cols = dot(after_mixer[stream].astype(BF16), mine)
-        finals.append((every, own_cols, dot(product, mine)))
+        finals.append((stream, every, own_cols, dot(product, mine)))
     with ns("update"):
         lax.fori_loop(0, own_rows, update, 0, unroll=UNROLL)
 
-    for stream, (every, own_cols, branch) in enumerate(finals):
+    for stream, every, own_cols, branch in finals:
         with ns("fin%d" % stream):
             every.wait_recv()
             for off in range(1, n_tp):
@@ -581,6 +596,19 @@
             every.wait_send()
         else:
             pl.when(cond)(every.wait_send)
+
+
+def finish(res_ref, state_ref, res_out, state_out, sem):
+    rows = state_ref.shape[0]
+    copies = [
+        pltpu.make_async_copy(state_ref.at[row], state_out.at[row], sem.at[row])
+        for row in range(rows)
+    ]
+    copies.append(pltpu.make_async_copy(res_ref, res_out, sem.at[rows]))
+    for copy in copies:
+        copy.start()
+    for copy in copies:
+        copy.wait()
 
 
 def place_back(rows, cols, peer):
@@ -686,7 +714,7 @@
     )
     vmem = pl.BlockSpec(memory_space=pltpu.VMEM)
     hbm = pl.BlockSpec(memory_space=pl.ANY)
-    return pl.pallas_call(
+    done = pl.pallas_call(
         functools.partial(kernel, n_kv, n_tp),
         out_shape=(
             pltpu.VMEM(residual_in.shape, BF16),
@@ -714,6 +742,18 @@
         ),
         name="layer",
     )(*small, delta_state, *big)
+    return pl.pallas_call(
+        finish,
+        out_shape=(
+            jax.ShapeDtypeStruct(residual_in.shape, BF16),
+            jax.ShapeDtypeStruct(delta_state.shape, F32),
+        ),
+        in_specs=[vmem, vmem],
+        out_specs=(hbm, hbm),
+        scratch_shapes=[pltpu.SemaphoreType.DMA((own_rows + 1,))],
+        compiler_params=pltpu.CompilerParams(vmem_limit_bytes=1024 * 1024),
+        name="finish",
+    )(*done)
 
 
 def solution(mesh):

time: 62.7 us -> 60.3 us (0.962)
  local copies, waits for them, and re-layouts: 2.62 us -> 0 us
    unnamed x2 -> x0, local copies, waits for them, and re-layouts: 2.62 us -> none
    pallas_call x0 -> x1, Pallas kernels: none -> 2.08 us  [body(): pl.pallas_call(finish, out_shape=(jax.ShapeDtypeStruct(residual_in.shape,...]
    pallas_call x1, Pallas kernels: 59.3 us -> 57.4 us  [body(): pl.pallas_call(functools.partial(kernel, n_kv, n_tp), out_shape=(pltpu.VM...]
where the time goes in v3:
time: 60.3 us; the launch traced here: 60.2 us
  Pallas kernels  59.5 us (99%)
  between operations  0.65 us (1%)
    pallas_call x1, Pallas kernels, body(): pl.pallas_call(functools.partial(kernel, n_kv, n_tp), out_shape=(pltpu.VM...  57.4 us
    pallas_call x1, Pallas kernels, body(): pl.pallas_call(finish, out_shape=(jax.ShapeDtypeStruct(residual_in.shape,...  2.08 us

profile of v3, /device:TPU:0, one launch (start us, length us, event | category | flops | bytes accessed | tf_op | source)
XLA Modules:
  0.0 60.2 jit_solution(3009544581780206831)
XLA Ops:
  0.6 57.4 %layer.1 = (bf16[64,64]{1,0:T(8,128)(2,1)S(1)}, f32[8,8,128,128]{3,2,1,0:T(8,128)S(1)}) custom-call(bf16[64,64]{1,0:T(8,128)(2,1)} %res_hbm.1, f32[1,256]{1,0:T(1,128)} %bitcast.10, f32[1,256]{1,0:T(1,128)} %bitcast.11, f32[1,256]{1,0:T(1,128)} %bitcast.12, bf16[32,256]{1,0:T(8,128)(2,1)} %bitcast.8, bf16[32,256]{1,0:T(8,128)(2,1)} %bitcast.9, ...), custom_call_target="tpu_custom_call" | custom-call | tf_op jit(solution)/shard_map/layer/pallas_call | solution.py:717
  58.1 2.1 %finish.1 = (bf16[64,64]{1,0:T(8,128)(2,1)}, f32[8,8,128,128]{3,2,1,0:T(8,128)}) custom-call(bf16[64,64]{1,0:T(8,128)(2,1)S(1)} %get-tuple-element.4.res_ref, f32[8,8,128,128]{3,2,1,0:T(8,128)S(1)} %get-tuple-element.5.state_ref), custom_call_target="tpu_custom_call" | custom-call | tf_op jit(solution)/shard_map/finish/pallas_call | solution.py:745

commit v4 on v3

--- a/solution.py
+++ b/solution.py
@@ -31,12 +31,6 @@
 
 def dot_first(a, b):
     return lax.dot_general(a, b, (((0,), (0,)), ((), ())), preferred_element_type=F32)
-
-
-def place(rows, cols, shift):
-    row = lax.broadcasted_iota(jnp.int32, (rows, cols), 0)
-    col = lax.broadcasted_iota(jnp.int32, (rows, cols), 1)
-    return jnp.where(col == row + shift, 1.0, 0.0).astype(F32).astype(BF16)
 
 
 def kernel(
@@ -65,7 +59,6 @@
     down2_hbm,
     res_out_ref,
     state,
-    res_ref,
     gain_first_ref,
     gain_mixer_ref,
     gain_second_ref,
@@ -105,7 +98,8 @@
     s2b,
     r2b,
     hid2,
-    fin_send,
+    kept_rows,
+    product,
     fin_recv,
     qk_rows,
     val_rows,
@@ -121,7 +115,7 @@
 ):
     kv = lax.axis_index("kv")
     tp = lax.axis_index("tp")
-    batch, piece = res_ref.shape
+    _, batch, piece = res_all.shape
     depth = gate1.shape[0]
     width = depth * n_kv
     own_rows = batch // n_kv
@@ -169,7 +163,7 @@
         pltpu.make_async_copy(src, dst, w_sem.at[i]) for i, (src, dst) in enumerate(weight_pairs)
     ]
     small_pairs = (
-        (res_hbm, res_ref),
+        (res_hbm, res_all.at[tp]),
         (gain_first_hbm, gain_first_ref),
         (gain_mixer_hbm, gain_mixer_ref),
         (gain_second_hbm, gain_second_ref),
@@ -404,7 +398,8 @@
         )
 
     smalls[0].wait()
-    every = send_tp(0, lambda off: res_ref, lambda off: res_all.at[tp], res_all.at[pl.ds(0, n_tp - 1)])
+    own = res_all.at[tp]
+    every = send_tp(0, lambda off: own, lambda off: own, res_all.at[pl.ds(0, n_tp - 1)])
     for load in loads[3:]:
         load.start()
     state_load = pltpu.make_async_copy(state_hbm, state, in_sem)
@@ -416,12 +411,10 @@
         dot_first(beta_ref[...], place_heads(beta_ref.shape[0], tp * heads, 0, heads))
         + dot_first(decay_ref[...], place_heads(beta_ref.shape[0], tp * heads, heads, heads))
     ).astype(BF16)
-    whole = dot(res_ref[...], place(piece, depth, tp * piece))
     with ns("tp_gather"):
         every.wait_recv()
-        for off in range(1, n_tp):
-            source = lax.rem(tp + n_tp - off, n_tp)
-            whole = whole + dot(res_all[source], place(piece, depth, source * piece))
+        pieces = [res_all[source].astype(F32) for source in range(n_tp)]
+        whole = jnp.concatenate(pieces, axis=1)
 
     first_bufs = (s1a, r1a, s1b, r1b)
     residual = [rows_of(whole, stream) for stream in range(2)]
@@ -534,6 +527,7 @@
             branch = join(shared, stream, parm)
         kept = (after_first[stream] + branch).astype(BF16).astype(F32)
         after_mixer[stream] = kept
+        kept_rows[stream] = kept
         with ns("f2_in"):
             ffn_in(16, stream, kept, gain_second_ref, gate2, up2, second_bufs)
 
@@ -559,32 +553,41 @@
         pl.when(owner)(functools.partial(ffn_mid, 16, 4, stream, second_bufs, hid2))
     ffn_sent(16, second_bufs, hid2)
     loads[10].wait()
+    tile = min(LANES, depth)
+    per = tile // piece
+
+    def tile_of(ref, stream, place):
+        if tile == depth:
+            return ref.at[stream]
+        return ref.at[stream, :, pl.ds(pl.multiple_of((place // per) * tile, tile), tile)]
+
     finals = []
-    mine = place_back(depth, piece, tp)
     for stream in ORDER:
         with ns("f2_ag%d" % stream):
             ffn_arrive(16, 4, stream, hid2)
-        product = dot(flat(hid2, stream), down2[...]).astype(BF16)
-        for off in range(1, n_tp):
-            peer = lax.rem(tp + off, n_tp)
-            fin_send[stream, off] = dot(product, place_back(depth, piece, peer)).astype(BF16)
+        product[stream] = dot(flat(hid2, stream), down2[...]).astype(BF16)
         every = send_tp(
             22 + stream,
-            lambda off: fin_send.at[stream, off],
+            lambda off: tile_of(product, stream, lax.rem(tp + off, n_tp)),
             lambda off: fin_recv.at[stream, off],
             fin_recv.at[stream, pl.ds(1, n_tp - 1)],
         )
-        own_cols = dot(after_mixer[stream].astype(BF16), mine)
-        finals.append((stream, every, own_cols, dot(product, mine)))
+        finals.append((stream, every))
+
     with ns("update"):
         lax.fori_loop(0, own_rows, update, 0, unroll=UNROLL)
 
-    for stream, every, own_cols, branch in finals:
+    for stream, every in finals:
         with ns("fin%d" % stream):
             every.wait_recv()
+            branch = tile_of(product, stream, tp)[...].astype(F32)
             for off in range(1, n_tp):
                 branch = branch + fin_recv[stream, off].astype(F32)
-        done = own_cols + 0.5 * branch
+        wide = tile_of(kept_rows, stream, tp)[...] + 0.5 * branch
+        done = wide[:, :piece]
+        for part in range(1, per):
+            mine = wide[:, part * piece : (part + 1) * piece]
+            done = jnp.where(lax.rem(tp, per) == part, mine, done)
         for j in range(half):
             start = start_of(stream, j)
             res_out_ref[start : start + own_rows] = done[j * own_rows : (j + 1) * own_rows].astype(
@@ -609,12 +612,6 @@
         copy.start()
     for copy in copies:
         copy.wait()
-
-
-def place_back(rows, cols, peer):
-    row = lax.broadcasted_iota(jnp.int32, (rows, cols), 0)
-    col = lax.broadcasted_iota(jnp.int32, (rows, cols), 1)
-    return jnp.where(row == col + peer * cols, 1.0, 0.0).astype(F32).astype(BF16)
 
 
 def place_heads(rows, first, lane_start, count):
@@ -722,12 +719,16 @@
         ),
         in_specs=[hbm] * (len(small) + 1 + len(big)),
         out_specs=(vmem, vmem),
-        scratch_shapes=[like(x) for x in (*small, *big)]
+        scratch_shapes=[like(x) for x in (*small[1:], *big)]
         + [pltpu.VMEM((n_tp, batch, piece), BF16)]
         + ffn_bufs
         + mixer_bufs
         + ffn_bufs[:-1]
-        + [pltpu.VMEM((2, n_tp, batch // 2, piece), BF16)] * 2
+        + [
+            pltpu.VMEM((2, batch // 2, depth), F32),
+            pltpu.VMEM((2, batch // 2, depth), BF16),
+            pltpu.VMEM((2, n_tp, batch // 2, min(LANES, depth)), BF16),
+        ]
         + [row_buf(2 * key_heads), row_buf(heads), row_buf(heads), row_buf(heads), row_buf(heads)]
         + [
             pltpu.SemaphoreType.DMA((len(big),)),

time: 60.3 us -> 60.1 us (level)
  no operation moved by 1% of the time
where the time goes in v4:
time: 60.1 us; the launch traced here: 59.9 us
  Pallas kernels  59.3 us (99%)
  between operations  0.65 us (1%)
    pallas_call x1, Pallas kernels, body(): pl.pallas_call(functools.partial(kernel, n_kv, n_tp), out_shape=(pltpu.VM...  57.2 us
    pallas_call x1, Pallas kernels, body(): pl.pallas_call(finish, out_shape=(jax.ShapeDtypeStruct(residual_in.shape,...  2.08 us

profile of v4, /device:TPU:0, one launch (start us, length us, event | category | flops | bytes accessed | tf_op | source)
XLA Modules:
  0.0 59.9 jit_solution(10327563813234979468)
XLA Ops:
  0.6 57.2 %layer.1 = (bf16[64,64]{1,0:T(8,128)(2,1)S(1)}, f32[8,8,128,128]{3,2,1,0:T(8,128)S(1)}) custom-call(bf16[64,64]{1,0:T(8,128)(2,1)} %res_hbm.1, f32[1,256]{1,0:T(1,128)} %bitcast.10, f32[1,256]{1,0:T(1,128)} %bitcast.11, f32[1,256]{1,0:T(1,128)} %bitcast.12, bf16[32,256]{1,0:T(8,128)(2,1)} %bitcast.8, bf16[32,256]{1,0:T(8,128)(2,1)} %bitcast.9, ...), custom_call_target="tpu_custom_call" | custom-call | tf_op jit(solution)/shard_map/layer/pallas_call | solution.py:714
  57.8 2.1 %finish.1 = (bf16[64,64]{1,0:T(8,128)(2,1)}, f32[8,8,128,128]{3,2,1,0:T(8,128)}) custom-call(bf16[64,64]{1,0:T(8,128)(2,1)S(1)} %get-tuple-element.4.res_ref, f32[8,8,128,128]{3,2,1,0:T(8,128)S(1)} %get-tuple-element.5.state_ref), custom_call_target="tpu_custom_call" | custom-call | tf_op jit(solution)/shard_map/finish/pallas_call | solution.py:746

commit v5 on v4

--- a/solution.py
+++ b/solution.py
@@ -214,6 +214,14 @@
 
     sent = []
 
+    def settle():
+        for cond, every in sent:
+            if cond is None:
+                every.wait_send()
+            else:
+                pl.when(cond)(every.wait_send)
+        sent.clear()
+
     def send_tp(event, src_of, dst_of, block):
         sems = send_sem.at[event], recv_sem.at[event]
         for off in range(1, n_tp):
@@ -513,6 +521,9 @@
             normed = reading * lax.rsqrt(mean + EPS) * head_gain_ref[...]
             nrm[my_j, :, cols] = (normed * out_gate[:, cols]).astype(BF16)
         spread(12, 2, nrm)
+        late_send = sent.pop()
+    settle()
+    sent.append(late_send)
 
     def mixer_out(stream):
         with ns("m_ag%d" % stream):
@@ -529,7 +540,7 @@
         after_mixer[stream] = kept
         kept_rows[stream] = kept
         with ns("f2_in"):
-            ffn_in(16, stream, kept, gain_second_ref, gate2, up2, second_bufs)
+            ffn_in(1, stream, kept, gain_second_ref, gate2, up2, second_bufs)
 
     for load in loads[7:10]:
         load.wait()
@@ -550,8 +561,8 @@
         return carry
 
     for stream in ORDER:
-        pl.when(owner)(functools.partial(ffn_mid, 16, 4, stream, second_bufs, hid2))
-    ffn_sent(16, second_bufs, hid2)
+        pl.when(owner)(functools.partial(ffn_mid, 1, 0, stream, second_bufs, hid2))
+    ffn_sent(1, second_bufs, hid2)
     loads[10].wait()
     tile = min(LANES, depth)
     per = tile // piece
@@ -564,16 +575,20 @@
     finals = []
     for stream in ORDER:
         with ns("f2_ag%d" % stream):
-            ffn_arrive(16, 4, stream, hid2)
+            ffn_arrive(1, 0, stream, hid2)
         product[stream] = dot(flat(hid2, stream), down2[...]).astype(BF16)
         every = send_tp(
-            22 + stream,
+            16 + stream,
             lambda off: tile_of(product, stream, lax.rem(tp + off, n_tp)),
             lambda off: fin_recv.at[stream, off],
             fin_recv.at[stream, pl.ds(1, n_tp - 1)],
         )
         finals.append((stream, every))
 
+    final_sends = sent[-2:]
+    del sent[-2:]
+    settle()
+    sent.extend(final_sends)
     with ns("update"):
         lax.fori_loop(0, own_rows, update, 0, unroll=UNROLL)
 
@@ -594,11 +609,7 @@
                 BF16
             )
 
-    for cond, every in sent:
-        if cond is None:
-            every.wait_send()
-        else:
-            pl.when(cond)(every.wait_send)
+    settle()
 
 
 def finish(res_ref, state_ref, res_out, state_out, sem):
@@ -734,9 +745,9 @@
             pltpu.SemaphoreType.DMA((len(big),)),
             pltpu.SemaphoreType.DMA((len(small),)),
             pltpu.SemaphoreType.DMA,
-            pltpu.SemaphoreType.DMA((24,)),
-            pltpu.SemaphoreType.DMA((24,)),
-            pltpu.SemaphoreType.DMA((6,)),
+            pltpu.SemaphoreType.DMA((18,)),
+            pltpu.SemaphoreType.DMA((18,)),
+            pltpu.SemaphoreType.DMA((4,)),
         ],
         compiler_params=pltpu.CompilerParams(
             collective_id=0, has_side_effects=True, vmem_limit_bytes=58 * 1024 * 1024

time: 60.1 us -> 59.9 us (level)
  no operation moved by 1% of the time
where the time goes in v5:
time: 59.9 us; the launch traced here: 59.8 us
  Pallas kernels  59.1 us (99%)
  between operations  0.65 us (1%)
    pallas_call x1, Pallas kernels, body(): pl.pallas_call(functools.partial(kernel, n_kv, n_tp), out_shape=(pltpu.VM...  57 us
    pallas_call x1, Pallas kernels, body(): pl.pallas_call(finish, out_shape=(jax.ShapeDtypeStruct(residual_in.shape,...  2.08 us

profile of v5, /device:TPU:0, one launch (start us, length us, event | category | flops | bytes accessed | tf_op | source)
XLA Modules:
  0.0 59.8 jit_solution(6814667335373903083)
XLA Ops:
  0.6 57.0 %layer.1 = (bf16[64,64]{1,0:T(8,128)(2,1)S(1)}, f32[8,8,128,128]{3,2,1,0:T(8,128)S(1)}) custom-call(bf16[64,64]{1,0:T(8,128)(2,1)} %res_hbm.1, f32[1,256]{1,0:T(1,128)} %bitcast.10, f32[1,256]{1,0:T(1,128)} %bitcast.11, f32[1,256]{1,0:T(1,128)} %bitcast.12, bf16[32,256]{1,0:T(8,128)(2,1)} %bitcast.8, bf16[32,256]{1,0:T(8,128)(2,1)} %bitcast.9, ...), custom_call_target="tpu_custom_call" | custom-call | tf_op jit(solution)/shard_map/layer/pallas_call | solution.py:725
  57.7 2.1 %finish.1 = (bf16[64,64]{1,0:T(8,128)(2,1)}, f32[8,8,128,128]{3,2,1,0:T(8,128)}) custom-call(bf16[64,64]{1,0:T(8,128)(2,1)S(1)} %get-tuple-element.4.res_ref, f32[8,8,128,128]{3,2,1,0:T(8,128)S(1)} %get-tuple-element.5.state_ref), custom_call_target="tpu_custom_call" | custom-call | tf_op jit(solution)/shard_map/finish/pallas_call | solution.py:757
